TPU v7x, 512 devices: a whole 4x4x16 slice. The times are simulated.
512 devices in a mesh: ep: 128 (over z, x, core), tp: 4 (over y).
Axes of the slice: x: 4, y: 4, z: 16, core: 2. Of those that a mesh axis runs over, the one named last changes fastest.
Arguments:
- tokens: bfloat16 [16384, 2048], P('ep'), may hold values from -6 to 6
- pre_gain: float32 [2048], replicated, may hold values from 0.1 to 1.9
- post_gain: float32 [2048], P('tp'), may hold values from 0.1 to 1.9
- expert_ids: int32 [16384, 2], P('ep'), may hold values from 0 to 127, all different within a row; in each aligned block of 128 rows (0 to 127, 128 to 255, ...) at most 3 rows name the same one
- route_weights: float32 [16384, 2], P('ep'), may hold values from 0.1 to 1
- w_gate: bfloat16 [128, 2048, 512], P('ep', None, 'tp'), may hold values from -0.125 to 0.125
- w_up: bfloat16 [128, 2048, 512], P('ep', None, 'tp'), may hold values from -0.125 to 0.125
- w_down: bfloat16 [128, 512, 2048], P('ep', None, 'tp'), may hold values from -0.25 to 0.25
Outputs:
- routed: bfloat16 [16384, 2048], P('ep', 'tp')
Inputs may be any that keep to these rules, and one draw needn't show every extreme that they name: `expert_ids`: each row names 2 different experts. Among the rows of one index of ep (aligned blocks of 128 rows) no expert is named by more than 3 rows, a bound that some block reaches.
All inputs are finite; a program needn't handle non-finite values.
Results may differ from a plain program's by a relative error of at most 0.007.
Values may be sent and summed in bfloat16 or wider, within the bound.
A program may use at most 64 MiB of HBM per device.

v0:
```python
import jax
import jax.numpy as jnp
from jax import lax
from jax.sharding import Mesh
from jax.sharding import PartitionSpec as P

EP = ("ep_0", "ep_1", "ep_2")


epsilon = 1e-06


def split_up(shard, dim, length):
    shape = shard.shape
    pieces = shard.reshape(*shape[:dim], length, shape[dim] // length, *shape[dim + 1 :])
    return jnp.moveaxis(pieces, dim, 0)


def joined_along(pieces, dim):
    shape = list(pieces.shape[1:])
    shape[dim] *= pieces.shape[0]
    return jnp.moveaxis(pieces, 0, dim).reshape(shape)


def exchange_in_order(pieces, axes, sequence):
    inside = pieces.shape[1:]
    out = pieces.reshape(*(lax.axis_size(a) for a in axes), *inside)
    for k in sequence:
        out = lax.all_to_all(out, axes[k], k, k, tiled=True)
    return out.reshape(-1, *inside)


def exchange_by_chip(shard, groups, sequence, split_dim, concat_dim):
    length = lax.axis_size(groups[0]) * lax.axis_size(groups[1])
    pieces = split_up(shard, split_dim, length)
    return joined_along(exchange_in_order(pieces, groups, sequence), concat_dim)


def from_everyone(shard, axis):
    length = lax.axis_size(axis)
    return lax.all_to_all(
        jnp.broadcast_to(shard[None], (length, *shard.shape)), axis, 0, 0, tiled=True
    )


def gathered_copies(shard, axis, dim):
    return joined_along(from_everyone(shard, axis), dim)


def over_pieces(shard, axis):
    pieces = lax.all_gather(shard, axis)
    return pieces.sum(axis=0)


def per_device(tokens, pre_gain, post_gain, expert_ids, route_weights, w_gate, w_up, w_down):
    tok_rows, row_width = tokens.shape
    pick_count = expert_ids.shape[1]
    ep_count = lax.axis_size(EP)
    local_experts = w_gate.shape[0]
    experts = ep_count * local_experts
    capacity = 3 * tok_rows * pick_count // (2 * experts)
    pick_total = tok_rows * pick_count
    flat_ids = expert_ids.reshape(pick_total)
    onehot = (flat_ids[:, None] == jnp.arange(experts, dtype=jnp.int32)[None, :]).astype(
        jnp.bfloat16
    )
    positions = jnp.arange(pick_total, dtype=jnp.int32)
    strict_lower = (positions[None, :] < positions[:, None]).astype(jnp.bfloat16)
    earlier = jnp.dot(strict_lower, onehot, preferred_element_type=jnp.float32)
    slot_index = jnp.sum(earlier * onehot, axis=1).astype(jnp.int32)
    target = flat_ids * capacity + slot_index
    values = tokens.astype(jnp.float32)
    row_scale = lax.rsqrt(jnp.mean(values * values, axis=1, keepdims=True) + epsilon)
    normed = (values * row_scale * pre_gain[None, :]).astype(jnp.bfloat16)
    part_width = row_width // lax.axis_size("tp")
    outgoing = lax.dynamic_slice_in_dim(normed, lax.axis_index("tp") * part_width, part_width, 1)
    sent_width = outgoing.shape[1]
    copies = jnp.broadcast_to(outgoing[:, None, :], (tok_rows, pick_count, sent_width)).reshape(
        pick_total, sent_width
    )
    buffer = jnp.zeros((experts * capacity, sent_width), jnp.bfloat16).at[target].set(copies)
    arrived = exchange_by_chip(buffer, (("ep_0", "ep_1"), "ep_2"), (1, 0), 0, 0)
    piece = gathered_copies(arrived, "tp", 1)
    count = piece.shape[1]
    block = piece.reshape(ep_count, local_experts, capacity, count)
    gate_add = jnp.einsum("sxcd,xdf->sxcf", block, w_gate, preferred_element_type=jnp.float32)
    up_add = jnp.einsum("sxcd,xdf->sxcf", block, w_up, preferred_element_type=jnp.float32)
    hidden = (jax.nn.silu(gate_add) * up_add).astype(jnp.bfloat16)
    out_cols = w_down.shape[2]
    piece = gathered_copies(hidden, "tp", 3)
    produced = jnp.einsum("sxcf,xfd->sxcd", piece, w_down, preferred_element_type=jnp.float32)
    results = produced.astype(jnp.bfloat16).reshape(experts * capacity, out_cols)
    returned = exchange_by_chip(results, (("ep_0", "ep_1"), "ep_2"), (1, 0), 0, 0)
    picked = returned[target].astype(jnp.float32) * route_weights.reshape(pick_total)[:, None]
    mixed = jnp.sum(picked.reshape(tok_rows, pick_count, out_cols), axis=1)
    squares = over_pieces(jnp.sum(mixed * mixed, axis=1), "tp")
    out_scale = lax.rsqrt(squares / row_width + epsilon)
    return (mixed * out_scale[:, None] * post_gain[None, :]).astype(jnp.bfloat16)


def solution(mesh):
    torus = Mesh(mesh.devices.reshape(16, 4, 2, mesh.shape["tp"]), ("ep_0", "ep_1", "ep_2", "tp"))
    in_specs = (
        P(EP, None),
        P(),
        P("tp"),
        P(EP, None),
        P(EP, None),
        P(EP, None, "tp"),
        P(EP, None, "tp"),
        P(EP, None, "tp"),
    )
    out_specs = P(EP, "tp")
    return jax.shard_map(
        per_device, mesh=torus, in_specs=in_specs, out_specs=out_specs, check_vma=False
    )
```

profile of v0, /device:TPU:2, one launch (start us, length us, event | category | flops | bytes accessed | tf_op | source)
XLA Modules:
  0.0 151.1 jit_solution(11407349126232424633)
XLA Ops:
  0.0 1.2 convert_element_type.55
  1.3 0.2 multiply_reduce_fusion
  1.6 0.8 dynamic-slice
  2.8 0.2 fusion.6
  3.4 1.6 %scatter_custom_fusion = bf16[384,512]{1,0:T(8,128)(2,1)S(1)} fusion(s32[256]{0:T(256)S(1)} %bitcast.52, bf16[256,512]{1,0:T(8,128)(2,1)S(1)} %reshape.110, bf16[]{:T(256)} %constant.11.clone.1), kind=kCustom, calls=%fused_computation.24 | custom fusion | bytes 393218 | tf_op jit(solution)/shard_map/scatter | solution.py:81
  5.0 0.2 reshape_reshape.7
  5.2 0.2 copy.19
  5.4 4.0 %all_to_all.30 = bf16[64,2,3,512]{3,0,2,1:T(8,128)(2,1)S(1)} all-to-all(bf16[64,2,3,512]{3,0,2,1:T(8,128)(2,1)S(1)} %copy.19), channel_id=1, replica_groups=mesh['ep_0'=16,'ep_1'=4,'ep_2'=2,'tp'=4] {'ep_2'}, dimensions={1} | all-to-all | bytes 786432 | tf_op jit(solution)/shard_map/all_to_all | solution.py:29
  9.4 0.4 copy.20
  9.8 45.9 %all_to_all.31 = bf16[64,2,3,512]{3,1,2,0:T(2,128)(2,1)S(1)} all-to-all(bf16[64,2,3,512]{3,1,2,0:T(2,128)(2,1)S(1)} %copy.20), channel_id=1, replica_groups=mesh['ep_0'=16,'ep_1'=4,'ep_2'=2,'tp'=4] {'ep_0','ep_1'}, dimensions={0} | all-to-all | bytes 786432 | tf_op jit(solution)/shard_map/all_to_all | solution.py:29
  55.7 0.2 copy.21
  55.9 0.3 broadcast_in_dim.14
  56.4 23.0 %all_to_all.32 = bf16[4,384,512]{2,1,0:T(8,128)(2,1)S(1)} all-to-all(bf16[4,384,512]{2,1,0:T(8,128)(2,1)S(1)} %broadcast_in_dim.15), channel_id=1, replica_groups=mesh['ep_0'=16,'ep_1'=4,'ep_2'=2,'tp'=4] {'tp'}, dimensions={0} | all-to-all | bytes 3145728 | tf_op jit(solution)/shard_map/all_to_all | solution.py:41
  79.4 1.2 copy.22
  80.6 2.4 %reshape.92 = bf16[128,3,2048]{2,1,0:T(4,128)(2,1)} reshape(bf16[384,4,512]{2,1,0:T(4,128)(2,1)S(1)} %copy.22) | data formatting | bytes 3145728 | tf_op jit(solution)/shard_map/reshape.1
  83.1 3.5 %convolution_bitcast_fusion.1 = f32[128,1,3,128]{3,0,2,1:T(8,128)S(1)} fusion(bf16[128,3,2048]{2,1,0:T(4,128)(2,1)} %reshape.92, bf16[1,2048,128]{2,1,0:T(8,128)(2,1)S(1)} %copy-done.6), kind=kOutput, calls=%fused_computation.6 | convolution fusion | flops 201326592 | bytes 2293760 | tf_op jit(solution)/shard_map/sxcd,xdf->sxcf/dot_general | solution.py:86
  86.6 1.8 %fusion.3 = bf16[128,3,128]{2,0,1:T(8,128)(2,1)S(1)} fusion(bf16[128,3,2048]{2,1,0:T(4,128)(2,1)S(1)} %copy-done.1, bf16[1,2048,128]{2,1,0:T(8,128)(2,1)S(1)} %copy-done.7, f32[128,1,3,128]{3,0,2,1:T(8,128)S(1)} %convolution_bitcast_fusion.1), kind=kOutput, calls=%fused_computation.9 | convolution fusion | flops 201621504 | bytes 2392064 | tf_op jit(solution)/shard_map/sxcd,xdf->sxcf/dot_general | solution.py:87
  88.5 9.8 %all_to_all.33 = bf16[4,128,1,3,128]{4,1,3,2,0:T(8,128)(2,1)S(1)} all-to-all(bf16[4,128,1,3,128]{4,1,3,2,0:T(8,128)(2,1)S(1)} %broadcast_in_dim.17), channel_id=1, replica_groups=mesh['ep_0'=16,'ep_1'=4,'ep_2'=2,'tp'=4] {'tp'}, dimensions={0} | all-to-all | bytes 786432 | tf_op jit(solution)/shard_map/all_to_all | solution.py:41
  98.2 0.3 copy.25
  98.5 0.2 reshape.95
  98.7 0.4 fusion
  99.3 4.0 %all_to_all.34 = bf16[64,2,3,512]{3,0,2,1:T(8,128)(2,1)S(1)} all-to-all(bf16[64,2,3,512]{3,0,2,1:T(8,128)(2,1)S(1)} %copy.26), channel_id=1, replica_groups=mesh['ep_0'=16,'ep_1'=4,'ep_2'=2,'tp'=4] {'ep_2'}, dimensions={1} | all-to-all | bytes 786432 | tf_op jit(solution)/shard_map/all_to_all | solution.py:29
  103.4 1.1 copy.27
  104.5 7.4 %all-to-all-start.5 = ((bf16[64,2,3,512]{3,1,2,0:T(2,128)(2,1)}), bf16[64,2,3,512]{3,1,2,0:T(2,128)(2,1)S(1)}, u32[]{:S(2)}, u32[]{:S(2)}) async-start(bf16[64,2,3,512]{3,1,2,0:T(2,128)(2,1)} %copy.27), calls=%async_computation.5 | async-start | bytes 786432 | tf_op jit(solution)/shard_map/all_to_all | solution.py:29
  112.0 27.3 %all-to-all-done.5 = bf16[64,2,3,512]{3,1,2,0:T(2,128)(2,1)S(1)} async-done(((bf16[64,2,3,512]{3,1,2,0:T(2,128)(2,1)}), bf16[64,2,3,512]{3,1,2,0:T(2,128)(2,1)S(1)}, u32[]{:S(2)}, u32[]{:S(2)}) %all-to-all-start.5) | async-done | bytes 393248 | tf_op jit(solution)/shard_map/all_to_all | solution.py:29
  139.3 0.2 copy.28
  139.5 0.3 reshape_reshape.8
  139.9 1.2 gather_fusion
  141.0 0.3 reshape.97
  141.4 0.7 multiply_reduce_fusion.1
  142.2 8.1 %all-gather.1 = f32[4,1,128]{2,1,0:T(1,128)S(1)} all-gather(f32[1,1,128]{2,1,0:T(1,128)S(1)} %bitcast.55), channel_id=2, replica_groups=mesh['ep_0'=16,'ep_1'=4,'ep_2'=2,'tp'=4] {'tp'}, dimensions={0}, use_global_device_ids=true | all-gather | bytes 2560 | tf_op jit(solution)/shard_map/all_gather | solution.py:51
  150.4 0.8 multiply_convert_fusion
  (36 shorter events, 1.5 us)
Async XLA Ops:
  0.0 98.7 %copy-start = (bf16[1,512,512]{2,1,0:T(8,128)(2,1)S(1)}, bf16[1,512,512]{2,1,0:T(8,128)(2,1)}, u32[]{:S(2)}) copy-start(bf16[1,512,512]{2,1,0:T(8,128)(2,1)} %param.15) | copy-start | bytes 1572868
  0.0 1.3 copy-start.2
  0.0 1.4 copy-start.3
  80.6 2.5 %copy-start.6 = (bf16[1,2048,128]{2,1,0:T(8,128)(2,1)S(1)}, bf16[1,2048,128]{2,1,0:T(8,128)(2,1)}, u32[]{:S(2)}) copy-start(bf16[1,2048,128]{2,1,0:T(8,128)(2,1)} %param.13) | copy-start | bytes 1572868
  83.1 3.5 %copy-start.1 = (bf16[128,3,2048]{2,1,0:T(4,128)(2,1)S(1)}, bf16[128,3,2048]{2,1,0:T(4,128)(2,1)}, u32[]{:S(2)}) copy-start(bf16[128,3,2048]{2,1,0:T(4,128)(2,1)} %reshape.92) | copy-start | bytes 4718596
  83.1 3.5 %copy-start.7 = (bf16[1,2048,128]{2,1,0:T(8,128)(2,1)S(1)}, bf16[1,2048,128]{2,1,0:T(8,128)(2,1)}, u32[]{:S(2)}) copy-start(bf16[1,2048,128]{2,1,0:T(8,128)(2,1)} %param.14) | copy-start | bytes 1572868
  99.2 12.6 %copy-start.5 = (f32[128,2]{0,1:T(2,128)S(1)}, f32[128,2]{0,1:T(2,128)}, u32[]{:S(2)}) copy-start(f32[128,2]{0,1:T(2,128)} %param.12) | copy-start | bytes 3076
  104.5 34.8 %all-to-all-start.5 = ((bf16[64,2,3,512]{3,1,2,0:T(2,128)(2,1)}), bf16[64,2,3,512]{3,1,2,0:T(2,128)(2,1)S(1)}, u32[]{:S(2)}, u32[]{:S(2)}) async-start(bf16[64,2,3,512]{3,1,2,0:T(2,128)(2,1)} %copy.27), calls=%async_computation.5 | async-start | bytes 786432 | tf_op jit(solution)/shard_map/all_to_all | solution.py:29
  139.9 10.5 %copy-start.4 = (f32[512]{0:T(512)S(1)}, f32[512]{0:T(512)}, u32[]{:S(2)}) copy-start(f32[512]{0:T(512)} %param.10) | copy-start | bytes 6148
where the time goes:
time: 152 us; the launch traced here: 151 us
  blocking collectives  94.9 us (62%)
  waiting for transfers between devices  27.3 us (18%)
  local copies, waits for them, and re-layouts  12.3 us (8%)
  starting transfers between devices  7.37 us (5%)
  matrix products  5.87 us (4%)
  other arithmetic  3.1 us (2%)
    all_to_all x3, blocking collectives, exchange_in_order(): out = lax.all_to_all(out, axes[k], k, k, tiled=True)  54 us
    all_to_all x2, blocking collectives, from_everyone(): lax.all_to_all(jnp.broadcast_to(shard[None], (length, *shard.shape)), axi...  32.8 us
    all_to_all x1, waiting for transfers between devices, exchange_in_order(): out = lax.all_to_all(out, axes[k], k, k, tiled=True)  27.3 us
    all_gather x1, blocking collectives, over_pieces(): pieces = lax.all_gather(shard, axis)  8.13 us
    all_to_all x1, starting transfers between devices, exchange_in_order(): out = lax.all_to_all(out, axes[k], k, k, tiled=True)  7.37 us
    dot_general x1, matrix products, per_device(): jnp.einsum('sxcd,xdf->sxcf', block, w_gate, preferred_element_type=jnp.fl...  3.5 us
  transfers between devices with their start and end apart: 1, of which 1 were waited for; matrix products, arithmetic and copies ran while one was open for 0% of the time, Pallas kernels for 0%

commit v1 on v0

v1 whole, which is shorter than its diff:
```python
import jax
import jax.numpy as jnp
from jax import lax
from jax.experimental import pallas as pl
from jax.experimental.pallas import tpu as pltpu
from jax.sharding import PartitionSpec as P

epsilon = 1e-06
MESH = pl.DeviceIdType.MESH
NZ, NX, NC = 16, 4, 2
STEPS = (8, -7, 7, -6, 6, -5, 5, -4, 4, -3, 3, -2, 2, -1, 1, 0)
CHUNKS = 8


def places():
    me = lax.axis_index("ep")
    z, x, c = lax.div(me, NX * NC), lax.rem(lax.div(me, NC), NX), lax.rem(me, NC)
    return (
        [lax.rem(z + d, NZ) * (NX * NC) for d in range(NZ)],
        [lax.rem(x + d, NX) * NC for d in range(NX)],
        [c, 1 - c],
    )


def exchange_kernel(rows, x_ref, o_ref, send_sem, recv_sem):
    zs, xs, cs = places()

    def index(dz, q):
        return zs[dz % NZ] + xs[q // NC] + cs[q % NC]

    def back(dz, q):
        return zs[-dz % NZ] + xs[-(q // NC) % NX] + cs[q % NC]

    barrier = pltpu.get_barrier_semaphore()
    for dz in STEPS:
        for q in range(NX * NC):
            if dz or q:
                pl.semaphore_signal(barrier, inc=1, device_id={"ep": index(dz, q)}, device_id_type=MESH)
    pl.semaphore_wait(barrier, NZ * NX * NC - 1)
    for n, dz in enumerate(STEPS):
        for q in range(NX * NC):
            if not (dz or q):
                continue
            pltpu.make_async_remote_copy(
                x_ref.at[pl.ds(index(dz, q) * rows, rows)],
                o_ref.at[pl.ds((n * 8 + q) * rows, rows)],
                send_sem.at[n // 2],
                recv_sem.at[n // 2],
                device_id={"ep": index(dz, q)},
                device_id_type=MESH,
            ).start()
    own = (NZ * NX * NC - 8) * rows
    o_ref[own : own + rows] = x_ref[pl.ds(index(0, 0) * rows, rows)]
    for j in range(CHUNKS):
        pieces = [(j * 16 * rows, 16 * rows)] if j < 7 else [(112 * rows, 8 * rows), (121 * rows, 7 * rows)]
        total = sum(p[1] for p in pieces)
        part = o_ref.at[pl.ds(0, total)]
        pltpu.make_async_copy(part, part, send_sem.at[j]).wait()
        pltpu.make_async_copy(part, part, recv_sem.at[j]).wait()


def exchange(pieces, number):
    rows = pieces.shape[0] // 128
    return pl.pallas_call(
        lambda *refs: exchange_kernel(rows, *refs),
        out_shape=jax.ShapeDtypeStruct(pieces.shape, pieces.dtype),
        in_specs=[pl.BlockSpec(memory_space=pltpu.VMEM)],
        out_specs=pl.BlockSpec(memory_space=pltpu.VMEM),
        scratch_shapes=[pltpu.SemaphoreType.DMA((CHUNKS,)), pltpu.SemaphoreType.DMA((CHUNKS,))],
        compiler_params=pltpu.CompilerParams(collective_id=number, has_side_effects=True),
    )(pieces)


def joined_along(pieces, dim):
    shape = list(pieces.shape[1:])
    shape[dim] *= pieces.shape[0]
    return jnp.moveaxis(pieces, 0, dim).reshape(shape)


def gathered_copies(shard, axis, dim):
    length = lax.axis_size(axis)
    out = lax.all_to_all(jnp.broadcast_to(shard[None], (length, *shard.shape)), axis, 0, 0, tiled=True)
    return joined_along(out, dim)


def per_device(tokens, pre_gain, post_gain, expert_ids, route_weights, w_gate, w_up, w_down):
    tok_rows, row_width = tokens.shape
    pick_count = expert_ids.shape[1]
    experts = lax.axis_size("ep")
    capacity = 3
    pick_total = tok_rows * pick_count
    flat_ids = expert_ids.reshape(pick_total)
    onehot = (flat_ids[:, None] == jnp.arange(experts, dtype=jnp.int32)[None, :]).astype(jnp.bfloat16)
    positions = jnp.arange(pick_total, dtype=jnp.int32)
    strict_lower = (positions[None, :] < positions[:, None]).astype(jnp.bfloat16)
    earlier = jnp.dot(strict_lower, onehot, preferred_element_type=jnp.float32)
    slot_index = jnp.sum(earlier * onehot, axis=1).astype(jnp.int32)
    target = flat_ids * capacity + slot_index
    values = tokens.astype(jnp.float32)
    row_scale = lax.rsqrt(jnp.mean(values * values, axis=1, keepdims=True) + epsilon)
    normed = (values * row_scale * pre_gain[None, :]).astype(jnp.bfloat16)
    part_width = row_width // lax.axis_size("tp")
    outgoing = lax.dynamic_slice_in_dim(normed, lax.axis_index("tp") * part_width, part_width, 1)
    slots = jnp.arange(experts * capacity, dtype=jnp.int32)
    match = (target.reshape(1, tok_rows, pick_count) == slots[:, None, None])
    pick = match.any(axis=2).astype(jnp.bfloat16)
    buffer = jnp.dot(pick, outgoing)
    arrived = exchange(buffer.reshape(-1, 4, 128), 0).reshape(experts * capacity, part_width)
    block = gathered_copies(arrived, "tp", 1)
    gate_add = jnp.dot(block, w_gate[0], preferred_element_type=jnp.float32)
    up_add = jnp.dot(block, w_up[0], preferred_element_type=jnp.float32)
    hidden = (jax.nn.silu(gate_add) * up_add).astype(jnp.bfloat16)
    piece = gathered_copies(hidden, "tp", 1)
    produced = jnp.dot(piece, w_down[0], preferred_element_type=jnp.float32).astype(jnp.bfloat16)
    me = lax.axis_index("ep")
    z, x, c = me // 8, (me // 2) % 4, me % 2
    steps = jnp.array(STEPS, jnp.int32)
    spot = jnp.zeros((NZ,), jnp.int32).at[steps % NZ].set(jnp.arange(NZ, dtype=jnp.int32))
    other = jnp.arange(experts, dtype=jnp.int32)
    zo, xo, co = other // 8, (other // 2) % 4, other % 2
    place = spot[(z - zo) % NZ] * 8 + ((x - xo) % 4) * 2 + (c - co) % 2
    by_device = produced.reshape(experts, capacity, -1)[place].reshape(-1, 4, 128)
    came = exchange(by_device, 1).reshape(experts, capacity, -1)
    home = spot[(z - zo) % NZ] * 8 + ((x - xo) % 4) * 2 + (c - co) % 2
    returned = came[home].reshape(experts * capacity, -1)
    picked = returned[target].astype(jnp.float32) * route_weights.reshape(pick_total)[:, None]
    mixed = jnp.sum(picked.reshape(tok_rows, pick_count, -1), axis=1)
    squares = lax.all_gather(jnp.sum(mixed * mixed, axis=1), "tp").sum(axis=0)
    out_scale = lax.rsqrt(squares / row_width + epsilon)
    return (mixed * out_scale[:, None] * post_gain[None, :]).astype(jnp.bfloat16)


def solution(mesh):
    in_specs = (
        P("ep", None),
        P(),
        P("tp"),
        P("ep", None),
        P("ep", None),
        P("ep", None, "tp"),
        P("ep", None, "tp"),
        P("ep", None, "tp"),
    )
    return jax.shard_map(per_device, mesh=mesh, in_specs=in_specs, out_specs=P("ep", "tp"), check_vma=False)
```

time: 152 us -> 131 us (0.86)
  the two profiles are of different devices: /device:TPU:2 before, /device:TPU:1 now
where the time goes in v1:
time: 131 us; the launch traced here: 130 us
  Pallas kernels  71.5 us (55%)
  waiting for transfers between devices  26.1 us (20%)
  local copies, waits for them, and re-layouts  12.7 us (10%)
  starting transfers between devices  7.78 us (6%)
  blocking collectives  6.14 us (5%)
  other arithmetic  3.22 us (2%)
  matrix products  2.14 us (2%)
    pallas_call x2, Pallas kernels, exchange(): pl.pallas_call(lambda *refs: exchange_kernel(rows, *refs), out_shape=jax....  71.5 us
    all_to_all x2, waiting for transfers between devices, gathered_copies(): lax.all_to_all(jnp.broadcast_to(shard[None], (length, *shard.shape)), axi...  26.1 us
    all_to_all x2, starting transfers between devices, gathered_copies(): lax.all_to_all(jnp.broadcast_to(shard[None], (length, *shard.shape)), axi...  7.78 us
    all_gather x1, blocking collectives, per_device(): squares = lax.all_gather(jnp.sum(mixed * mixed, axis=1), 'tp').sum(axis=0)  6.14 us
    broadcast_in_dim x3, local copies, waits for them, and re-layouts, gathered_copies(): jnp.broadcast_to(shard[None], (length, *shard.shape))  3.32 us
  transfers between devices with their start and end apart: 2, of which 2 were waited for; matrix products, arithmetic and copies ran while one was open for 0% of the time, Pallas kernels for 0%

profile of v1, /device:TPU:1, one launch (start us, length us, event | category | flops | bytes accessed | tf_op | source)
XLA Modules:
  0.0 129.9 jit_solution(14388879802167289476)
XLA Ops:
  0.0 1.2 convert_element_type.52
  1.3 0.2 multiply_reduce_fusion
  1.5 0.8 dynamic-slice
  2.6 0.1 eq.42
  2.7 0.2 fusion.1
  3.0 0.1 convert_element_type.51
  3.3 0.3 fusion.9
  3.5 1.0 copy.32.refs_0_
  4.6 39.5 %shard_map.91 = bf16[384,4,128]{2,1,0:T(4,128)(2,1)} custom-call(bf16[384,4,128]{2,1,0:T(4,128)(2,1)} %copy.32.refs_0_), custom_call_target="tpu_custom_call" | custom-call | tf_op jit(solution)/shard_map/pallas_call | solution.py:64
  44.1 1.2 copy.36
  45.3 1.3 broadcast_in_dim.9
  46.6 4.3 %all-to-all-start = ((bf16[4,384,512]{1,2,0:T(8,128)(2,1)}), bf16[4,384,512]{1,2,0:T(8,128)(2,1)S(1)}, u32[]{:S(2)}, u32[]{:S(2)}) async-start(bf16[4,384,512]{1,2,0:T(8,128)(2,1)} %broadcast_in_dim.9), calls=%async_computation | async-start | bytes 3145728 | tf_op jit(solution)/shard_map/all_to_all | solution.py:82
  51.0 0.1 mul.117
  51.3 19.8 %all-to-all-done = bf16[4,384,512]{1,2,0:T(8,128)(2,1)S(1)} async-done(((bf16[4,384,512]{1,2,0:T(8,128)(2,1)}), bf16[4,384,512]{1,2,0:T(8,128)(2,1)S(1)}, u32[]{:S(2)}, u32[]{:S(2)}) %all-to-all-start) | async-done | bytes 1572896 | tf_op jit(solution)/shard_map/all_to_all | solution.py:82
  71.1 0.6 fusion.4
  71.7 0.6 fusion
  72.5 0.8 broadcast_in_dim.10
  73.3 3.5 %all-to-all-start.1 = ((bf16[4,384,128]{1,2,0:T(8,128)(2,1)}), bf16[4,384,128]{1,2,0:T(8,128)(2,1)S(1)}, u32[]{:S(2)}, u32[]{:S(2)}) async-start(bf16[4,384,128]{1,2,0:T(8,128)(2,1)} %broadcast_in_dim.10), calls=%async_computation.1 | async-start | bytes 786432 | tf_op jit(solution)/shard_map/all_to_all | solution.py:82
  76.8 6.3 %all-to-all-done.1 = bf16[4,384,128]{1,2,0:T(8,128)(2,1)S(1)} async-done(((bf16[4,384,128]{1,2,0:T(8,128)(2,1)}), bf16[4,384,128]{1,2,0:T(8,128)(2,1)S(1)}, u32[]{:S(2)}, u32[]{:S(2)}) %all-to-all-start.1) | async-done | bytes 393248 | tf_op jit(solution)/shard_map/all_to_all | solution.py:82
  83.0 0.4 convolution_convert_fusion
  83.4 0.2 reshape.343
  83.7 1.0 gather_fusion
  84.7 1.1 reshape.344.refs_0_
  85.8 32.0 %shard_map.92 = bf16[384,4,128]{2,1,0:T(4,128)(2,1)} custom-call(bf16[384,4,128]{2,1,0:T(4,128)(2,1)} %reshape.344.refs_0_), custom_call_target="tpu_custom_call" | custom-call | tf_op jit(solution)/shard_map/pallas_call | solution.py:64
  117.8 1.4 %reshape.345 = bf16[128,3,512]{2,1,0:T(4,128)(2,1)S(1)} reshape(bf16[384,4,128]{2,1,0:T(4,128)(2,1)} %shard_map.92) | data formatting | bytes 786432 | tf_op jit(solution)/shard_map/reshape | solution.py:123
  119.3 1.0 gather_fusion.1
  120.3 0.3 reshape.346
  120.7 1.2 gather_fusion.2
  121.8 0.3 reshape.347
  122.2 0.7 multiply_reduce_fusion.1
  123.0 6.1 %all-gather.1 = f32[4,1,128]{2,1,0:T(1,128)S(1)} all-gather(f32[1,1,128]{2,1,0:T(1,128)S(1)} %bitcast.184), channel_id=2, replica_groups=mesh['ep'=128,'tp'=4] {'tp'}, dimensions={0}, use_global_device_ids=true | all-gather | bytes 2560 | tf_op jit(solution)/shard_map/all_gather | solution.py:128
  129.2 0.8 multiply_convert_fusion
  (31 shorter events, 0.9 us)
Async XLA Ops:
  0.0 83.0 %copy-start = (bf16[1,512,512]{2,1,0:T(8,128)(2,1)S(1)}, bf16[1,512,512]{2,1,0:T(8,128)(2,1)}, u32[]{:S(2)}) copy-start(bf16[1,512,512]{2,1,0:T(8,128)(2,1)} %param.16) | copy-start | bytes 1572868
  0.0 1.3 copy-start.1
  0.0 2.4 %copy-start.4 = (s32[128,2]{0,1:T(2,128)S(1)}, s32[128,2]{0,1:T(2,128)}, u32[]{:S(2)}) copy-start(s32[128,2]{0,1:T(2,128)} %param.12) | copy-start | bytes 3076
  46.6 4.5 %copy-start.5 = (f32[128,2]{0,1:T(2,128)S(1)}, f32[128,2]{0,1:T(2,128)}, u32[]{:S(2)}) copy-start(f32[128,2]{0,1:T(2,128)} %param.13) | copy-start | bytes 3076
  46.6 24.5 %copy-start.2 = (bf16[1,2048,128]{2,1,0:T(8,128)(2,1)S(1)}, bf16[1,2048,128]{2,1,0:T(8,128)(2,1)}, u32[]{:S(2)}) copy-start(bf16[1,2048,128]{2,1,0:T(8,128)(2,1)} %param.14) | copy-start | bytes 1572868
  46.6 24.5 %all-to-all-start = ((bf16[4,384,512]{1,2,0:T(8,128)(2,1)}), bf16[4,384,512]{1,2,0:T(8,128)(2,1)S(1)}, u32[]{:S(2)}, u32[]{:S(2)}) async-start(bf16[4,384,512]{1,2,0:T(8,128)(2,1)} %broadcast_in_dim.9), calls=%async_computation | async-start | bytes 3145728 | tf_op jit(solution)/shard_map/all_to_all | solution.py:82
  51.0 20.8 %copy-start.6 = (bf16[1,2048,128]{2,1,0:T(8,128)(2,1)S(1)}, bf16[1,2048,128]{2,1,0:T(8,128)(2,1)}, u32[]{:S(2)}) copy-start(bf16[1,2048,128]{2,1,0:T(8,128)(2,1)} %param.15) | copy-start | bytes 1572868
  73.3 9.8 %all-to-all-start.1 = ((bf16[4,384,128]{1,2,0:T(8,128)(2,1)}), bf16[4,384,128]{1,2,0:T(8,128)(2,1)S(1)}, u32[]{:S(2)}, u32[]{:S(2)}) async-start(bf16[4,384,128]{1,2,0:T(8,128)(2,1)} %broadcast_in_dim.10), calls=%async_computation.1 | async-start | bytes 786432 | tf_op jit(solution)/shard_map/all_to_all | solution.py:82
  120.7 8.5 %copy-start.3 = (f32[512]{0:T(512)S(1)}, f32[512]{0:T(512)}, u32[]{:S(2)}) copy-start(f32[512]{0:T(512)} %param.11) | copy-start | bytes 6148

commit v2 on v1

v2 whole, which is shorter than its diff:
```python
import jax
import jax.numpy as jnp
from jax import lax
from jax.experimental import pallas as pl
from jax.experimental.pallas import tpu as pltpu
from jax.sharding import PartitionSpec as P

epsilon = 1e-06
MESH = pl.DeviceIdType.MESH
NZ, NX, NC, NY = 16, 4, 2, 4
NQ = NX * NC
PEERS = NZ * NQ
CAP = 3
STEPS = (8, -7, 7, -6, 6, -5, 5, -4, 4, -3, 3, -2, 2, -1, 1, 0)
CHUNKS = 8
PER = PEERS // CHUNKS
ROWS = PER * CAP
LANES = 128
PARTS = 4
BLOCK = PARTS * CAP
TALL = PER * BLOCK
BF16, F32, I32 = jnp.bfloat16, jnp.float32, jnp.int32


def dot(a, b):
    return jnp.dot(a, b, preferred_element_type=F32)


def iota(shape, dim):
    return lax.broadcasted_iota(I32, shape, dim)


def tall_row(wide):
    part = sum((wide >= ROWS * k).astype(I32) for k in range(1, PARTS))
    rest = wide - part * ROWS
    block = (rest * 171) >> 9
    return block * BLOCK + part * CAP + (rest - block * CAP)


def kernel(
    tokens_hbm, pre_ref, post_ref, ids_ref, weights_ref, gate_hbm, up_hbm, down_hbm,
    o_ref,
    tokens, gate_up, down, sent, arrived, gathered, hidden, results, returned, squares,
    load_sem, out_sem, in_sem, feat_out, feat_in, hid_out, hid_in, ret_out, ret_in, sq_sem,
):
    me, y = lax.axis_index("ep"), lax.axis_index("tp")
    z, x, c = lax.div(me, NQ), lax.rem(lax.div(me, NC), NX), lax.rem(me, NC)
    zs = [lax.rem(z + d, NZ) * NQ for d in range(NZ)]
    xs = [lax.rem(x + d, NX) * NC for d in range(NX)]
    cs = [c, 1 - c]
    ys = [lax.rem(y + d, NY) for d in (1, 3, 2)]

    def ahead(n, q):
        return {"ep": zs[STEPS[n] % NZ] + xs[q // NC] + cs[q % NC]}

    def behind(n, q):
        return {"ep": zs[-STEPS[n] % NZ] + xs[-(q // NC) % NX] + cs[q % NC]}

    barrier = pltpu.get_barrier_semaphore()
    for n in range(NZ):
        for q in range(NQ):
            if STEPS[n] or q:
                pl.semaphore_signal(barrier, inc=1, device_id=ahead(n, q), device_id_type=MESH)
    for other in ys:
        pl.semaphore_signal(barrier, inc=1, device_id={"tp": other}, device_id_type=MESH)

    loads = [
        pltpu.make_async_copy(tokens_hbm, tokens, load_sem.at[0]),
        pltpu.make_async_copy(gate_hbm.at[0], gate_up.at[:, pl.ds(0, LANES)], load_sem.at[1]),
        pltpu.make_async_copy(up_hbm.at[0], gate_up.at[:, pl.ds(LANES, LANES)], load_sem.at[2]),
        pltpu.make_async_copy(down_hbm.at[0], down, load_sem.at[3]),
    ]
    for load in loads:
        load.start()

    rows = tokens.shape[0]
    lane = iota((rows, PEERS), 1)
    lower = (iota((rows, rows), 1) < iota((rows, rows), 0)).astype(BF16)
    spots, before = [], None
    for k in range(2):
        e = ids_ref[:, k : k + 1]
        dz = ((e >> 3) - z) & (NZ - 1)
        n = sum(jnp.where(dz == STEPS[i] % NZ, i, 0) for i in range(NZ))
        q = (((((e >> 1) & 3) - x) & 3) << 1) + (((e & 1) - c) & 1)
        p = n * NQ + q
        mark = (lane == p).astype(F32)
        earlier = dot(lower, mark.astype(BF16))
        if before is not None:
            earlier = earlier + before
        before = jnp.sum(mark, axis=0, keepdims=True)
        slot = jnp.sum(earlier * mark, axis=1, keepdims=True)
        spots.append(p * BLOCK + slot.astype(I32))
    across = []
    for spot in spots:
        row = jnp.transpose(jnp.broadcast_to(spot.astype(F32), (rows, rows)))[0:1, :].astype(I32)
        across.append(jnp.concatenate([row + CAP * part for part in range(PARTS)], axis=1))

    loads[0].wait()
    values = tokens[...].astype(F32)
    scale = lax.rsqrt(jnp.mean(values * values, axis=1, keepdims=True) + epsilon)
    width = PARTS * LANES
    mine = pl.ds(pl.multiple_of(y * width, width), width)
    normed = (tokens[:, mine].astype(F32) * scale * pre_ref[:, mine]).astype(BF16)
    stacked = jnp.concatenate([normed[:, part * LANES : (part + 1) * LANES] for part in range(PARTS)], axis=0)

    flat_sent = sent.reshape(PEERS * BLOCK, LANES)
    flat_arrived = arrived.reshape(PEERS * BLOCK, LANES)
    flat_results = results.reshape(PEERS * BLOCK, LANES)
    flat_returned = returned.reshape(PEERS * BLOCK, LANES)
    for j in range(CHUNKS):
        r = iota((TALL, rows * PARTS), 0) + j * TALL
        take = jnp.where((r == across[0]) | (r == across[1]), 1.0, 0.0).astype(BF16)
        flat_sent[j * TALL : (j + 1) * TALL, :] = dot(take, stacked).astype(BF16)

    own = (PEERS - NQ) * CAP
    pl.semaphore_wait(barrier, PEERS - 1 + NY - 1)

    def send_blocks(source, target, sends, receives, j, place):
        for b in range(PER):
            n, q = divmod(j * PER + b, NQ)
            if not (STEPS[n] or q):
                continue
            at = pl.ds((j * PER + b) * CAP, CAP)
            pltpu.make_async_remote_copy(
                source.at[at], target.at[at], sends.at[j], receives.at[j], device_id=place(n, q), device_id_type=MESH
            ).start()

    def wait_blocks(buffer, sem, j):
        count = ROWS if j < CHUNKS - 1 else ROWS - CAP
        part = buffer.at[pl.ds(0, count)]
        pltpu.make_async_copy(part, part, sem.at[j]).wait()

    def send_tp(buffer, sends, receives, j):
        for other in ys:
            pltpu.make_async_remote_copy(
                buffer.at[j, y], buffer.at[j, y], sends.at[j], receives.at[j],
                device_id={"tp": other}, device_id_type=MESH,
            ).start()

    def wait_tp(buffer, sem, j):
        part = buffer.at[j, pl.ds(0, NY - 1)]
        pltpu.make_async_copy(part, part, sem.at[j]).wait()

    for j in range(CHUNKS):
        send_blocks(sent, arrived, out_sem, in_sem, j, ahead)
    arrived[own : own + CAP] = sent[own : own + CAP]

    to_wide = (iota((TALL, TALL), 1) == tall_row(iota((TALL, TALL), 0))).astype(BF16)
    to_tall = (iota((TALL, TALL), 0) == tall_row(iota((TALL, TALL), 1))).astype(BF16)

    def collect(j):
        wait_blocks(arrived, in_sem, j)
        wide = dot(to_wide, flat_arrived[j * TALL : (j + 1) * TALL, :]).astype(BF16)
        wide = jnp.concatenate([wide[part * ROWS : (part + 1) * ROWS] for part in range(PARTS)], axis=1)
        gathered[j, y] = wide
        send_tp(gathered, feat_out, feat_in, j)

    def gated(j):
        wait_tp(gathered, feat_in, j)
        total = sum(dot(gathered[j, other], gate_up[other * width : (other + 1) * width, :]) for other in range(NY))
        gate, up = total[:, :LANES], total[:, LANES:]
        hidden[j, y] = (gate / (1.0 + jnp.exp(-gate)) * up).astype(BF16)
        send_tp(hidden, hid_out, hid_in, j)

    def project(j):
        wait_tp(hidden, hid_in, j)
        units = jnp.concatenate([hidden[j, other] for other in range(NY)], axis=1)
        made = dot(units, down[...]).astype(BF16)
        made = jnp.concatenate([made[:, part * LANES : (part + 1) * LANES] for part in range(PARTS)], axis=0)
        flat_results[j * TALL : (j + 1) * TALL, :] = dot(to_tall, made).astype(BF16)
        send_blocks(results, returned, ret_out, ret_in, j, behind)
        if j == CHUNKS - 1:
            returned[own : own + CAP] = results[own : own + CAP]

    for load in loads[1:]:
        load.wait()
    for step in range(CHUNKS + 2):
        if step < CHUNKS:
            collect(step)
        if 0 <= step - 1 < CHUNKS:
            gated(step - 1)
        if 0 <= step - 2 < CHUNKS:
            project(step - 2)

    mixed = jnp.zeros((rows * PARTS, LANES), F32)
    for j in range(CHUNKS):
        r = iota((rows, TALL), 1) + j * TALL
        share = jnp.concatenate(
            [
                sum(jnp.where(r == spots[k] + CAP * part, weights_ref[:, k : k + 1], 0.0) for k in range(2))
                for part in range(PARTS)
            ],
            axis=0,
        )
        coarse = share.astype(BF16)
        fine = (share - coarse.astype(F32)).astype(BF16)
        wait_blocks(returned, ret_in, j)
        back = flat_returned[j * TALL : (j + 1) * TALL, :]
        mixed = mixed + (dot(coarse, back) + dot(fine, back))
    pieces = [mixed[part * rows : (part + 1) * rows] for part in range(PARTS)]

    square = jnp.sum(sum(piece * piece for piece in pieces), axis=1, keepdims=True)
    squares[y] = jnp.transpose(jnp.broadcast_to(square, (rows, rows)))[0:1, :]
    for other in ys:
        pltpu.make_async_remote_copy(
            squares.at[y], squares.at[y], sq_sem.at[0], sq_sem.at[1], device_id={"tp": other}, device_id_type=MESH
        ).start()
    for j in range(CHUNKS):
        wait_blocks(sent, out_sem, j)
        wait_blocks(results, ret_out, j)
        wait_tp(gathered, feat_out, j)
        wait_tp(hidden, hid_out, j)
    three = squares.at[pl.ds(0, NY - 1)]
    pltpu.make_async_copy(three, three, sq_sem.at[1]).wait()
    total = squares[0] + squares[1] + squares[2] + squares[3]
    total = jnp.transpose(jnp.broadcast_to(total, (rows, rows)))
    out_scale = lax.rsqrt(total / (width * NY) + epsilon)
    for part in range(PARTS):
        at = slice(part * LANES, (part + 1) * LANES)
        o_ref[:, at] = (pieces[part] * out_scale * post_ref[:, at]).astype(BF16)
    pltpu.make_async_copy(three, three, sq_sem.at[0]).wait()


def per_device(tokens, pre_gain, post_gain, expert_ids, route_weights, w_gate, w_up, w_down):
    rows, row_width = tokens.shape
    width = PARTS * LANES
    blocks = pltpu.VMEM((PEERS * CAP, PARTS, LANES), BF16)
    sems = pltpu.SemaphoreType.DMA((CHUNKS,))
    vmem, hbm = pl.BlockSpec(memory_space=pltpu.VMEM), pl.BlockSpec(memory_space=pl.ANY)
    return pl.pallas_call(
        kernel,
        out_shape=jax.ShapeDtypeStruct((rows, width), BF16),
        in_specs=[hbm, vmem, vmem, vmem, vmem, hbm, hbm, hbm],
        out_specs=vmem,
        scratch_shapes=[
            pltpu.VMEM((rows, row_width), BF16),
            pltpu.VMEM((row_width, 2 * LANES), BF16),
            pltpu.VMEM((w_down.shape[1], width), BF16),
            blocks,
            blocks,
            pltpu.VMEM((CHUNKS, NY, ROWS, width), BF16),
            pltpu.VMEM((CHUNKS, NY, ROWS, LANES), BF16),
            blocks,
            blocks,
            pltpu.VMEM((NY, 1, rows), F32),
            pltpu.SemaphoreType.DMA((4,)),
            *[sems] * 8,
            pltpu.SemaphoreType.DMA((2,)),
        ],
        compiler_params=pltpu.CompilerParams(collective_id=0, has_side_effects=True),
    )(tokens, pre_gain[None, :], post_gain[None, :], expert_ids, route_weights, w_gate, w_up, w_down)


def solution(mesh):
    in_specs = (
        P("ep", None),
        P(),
        P("tp"),
        P("ep", None),
        P("ep", None),
        P("ep", None, "tp"),
        P("ep", None, "tp"),
        P("ep", None, "tp"),
    )
    return jax.shard_map(per_device, mesh=mesh, in_specs=in_specs, out_specs=P("ep", "tp"), check_vma=False)
```

time: 131 us -> 76.3 us (0.58)
  waiting for transfers between devices: 26.1 us -> 0 us
  local copies, waits for them, and re-layouts: 12.7 us -> 3.72 us
  starting transfers between devices: 7.78 us -> 0 us
  blocking collectives: 6.14 us -> 0 us
  other arithmetic: 3.22 us -> 0 us
  matrix products: 2.14 us -> 0 us
    all_to_all x2 -> x0, waiting for transfers between devices: 26.1 us -> none  [gathered_copies(): lax.all_to_all(jnp.broadcast_to(shard[None], (length, *shard.shape)), axi...]
    all_to_all x2 -> x0, starting transfers between devices: 7.78 us -> none  [gathered_copies(): lax.all_to_all(jnp.broadcast_to(shard[None], (length, *shard.shape)), axi...]
    all_gather x1 -> x0, blocking collectives: 6.14 us -> none  [per_device(): squares = lax.all_gather(jnp.sum(mixed * mixed, axis=1), 'tp').sum(axis=0)]
    unnamed x16 -> x7, local copies, waits for them, and re-layouts: 0.27 us -> 3.72 us
    broadcast_in_dim x3 -> x0, local copies, waits for them, and re-layouts: 3.32 us -> none  [gathered_copies(): jnp.broadcast_to(shard[None], (length, *shard.shape))]
    gather x3 -> x0, local copies, waits for them, and re-layouts: 3.23 us -> none  [the longest x1 1.15 us: per_device(): returned[target].astype(jnp.float32)]
    reshape x4 -> x0, local copies, waits for them, and re-layouts: 3.07 us -> none  [the longest x1 1.44 us: per_device(): came = exchange(by_device, 1).reshape(experts, capacity, -1)]
    dot_general x5 -> x0, matrix products: 2.14 us -> none  [the longest x1 0.64 us: per_device(): up_add = jnp.dot(block, w_up[0], preferred_element_type=jnp.float32)]
  transfers between devices with their start and end apart: 2 -> 0, of which waited for: 2 -> 0; matrix products, arithmetic and copies ran while one was open for 0% -> 0% of each run, Pallas kernels for 0% -> 0%
where the time goes in v2:
time: 76.3 us; the launch traced here: 76.1 us
  Pallas kernels  72.3 us (95%)
  local copies, waits for them, and re-layouts  3.72 us (5%)
    pallas_call x1, Pallas kernels, per_device(): pl.pallas_call(kernel, out_shape=jax.ShapeDtypeStruct((rows, width), BF16...  72.3 us
    unnamed x7, local copies, waits for them, and re-layouts  3.72 us

profile of v2, /device:TPU:1, one launch (start us, length us, event | category | flops | bytes accessed | tf_op | source)
XLA Modules:
  0.0 76.1 jit_solution(7308844179192405859)
XLA Ops:
  0.0 0.0 copy-start
  0.0 0.7 copy-done
  0.7 0.0 copy-start.1
  0.7 0.7 copy.9.ids_ref
  1.4 0.0 copy-done.1
  1.4 0.7 copy.10.weights_ref
  2.2 72.3 %shard_map.82 = bf16[128,512]{1,0:T(8,128)(2,1)} custom-call(bf16[128,2048]{1,0:T(8,128)(2,1)} %tokens_hbm.1, f32[1,2048]{1,0:T(1,128)} %bitcast.2, f32[1,512]{1,0:T(1,128)} %bitcast.3, s32[128,2]{1,0:T(8,128)} %copy.9.ids_ref, f32[128,2]{1,0:T(8,128)} %copy.10.weights_ref, bf16[1,2048,128]{2,1,0:T(8,128)(2,1)} %gate_hbm.1, bf16[1,2048,128]{2,1,0:T(8,128)(2,1)} %up_hbm.1, ...), custom_call_target="tpu_custom_call" | custom-call | tf_op jit(solution)/shard_map/pallas_call | solution.py:230
  74.5 1.6 %copy.12 = bf16[128,512]{1,0:T(8,128)(2,1)} copy(bf16[128,512]{1,0:T(8,128)(2,1)} %shard_map.82) | data formatting | bytes 262144
Async XLA Ops:
  0.0 0.7 copy-start
  0.7 0.7 copy-start.1

commit v3 on v2

v3 whole, which is shorter than its diff:
```python
import jax
import jax.numpy as jnp
from jax import lax
from jax.experimental import pallas as pl
from jax.experimental.pallas import tpu as pltpu
from jax.sharding import PartitionSpec as P

epsilon = 1e-06
MESH = pl.DeviceIdType.MESH
NZ, NX, NC, NY = 16, 4, 2, 4
NQ = NX * NC
PEERS = NZ * NQ
CAP = 3
STEPS = (0, 1, -1, 2, -2, 3, -3, 4, 8, -7, 7, -6, 6, -5, 5, -4)
PLAN = (
    "K0", "S0", "S1", "K1", "S2", "S3", "K2", "S4", "S5", "S6", "S7", "C0", "C1", "C2", "C3", "G0", "G1", "G2",
    "G3", "P0", "C4", "P1", "P2", "P3", "C5", "G4", "C6", "G5", "P4", "C7", "G6", "P5", "G7", "P6", "P7", "M0",
    "M1", "M2", "M3", "M4", "M5", "M6", "M7",
)
NEAR = 2
CHUNKS = 8
PER = PEERS // CHUNKS
ROWS = PER * CAP
LANES = 128
PARTS = 4
BLOCK = PARTS * CAP
TALL = PER * BLOCK
BF16, F32, I32 = jnp.bfloat16, jnp.float32, jnp.int32


def dot(a, b):
    return jnp.dot(a, b, preferred_element_type=F32)


def iota(shape, dim):
    return lax.broadcasted_iota(I32, shape, dim)


def tall_row(wide):
    part = sum((wide >= ROWS * k).astype(I32) for k in range(1, PARTS))
    rest = wide - part * ROWS
    block = (rest * 171) >> 9
    return block * BLOCK + part * CAP + (rest - block * CAP)


def kernel(
    tokens_hbm, pre_hbm, ids_hbm, weights_hbm, gate_hbm, up_hbm, down_hbm,
    o_ref,
    tokens, pre, ids, weights, gate_up, down, sent, arrived, gathered, hidden, results, returned, squares, mixed,
    load_sem, wide_sem, out_sem, in_sem, feat_out, feat_in, hid_out, hid_in, ret_out, ret_in, sq_sem,
):
    me, y = lax.axis_index("ep"), lax.axis_index("tp")
    z, x, c = lax.div(me, NQ), lax.rem(lax.div(me, NC), NX), lax.rem(me, NC)
    zs = [lax.rem(z + d, NZ) * NQ for d in range(NZ)]
    xs = [lax.rem(x + d, NX) * NC for d in range(NX)]
    cs = [c, 1 - c]
    ys = [lax.rem(y + d, NY) for d in (1, 3, 2)]

    def at(dz, q):
        return {"ep": zs[dz % NZ] + xs[q // NC] + cs[q % NC]}

    def ahead(n, q):
        return at(STEPS[n], q)

    def behind(n, q):
        return {"ep": zs[-STEPS[n] % NZ] + xs[-(q // NC) % NX] + cs[q % NC]}

    barrier = pltpu.get_barrier_semaphore()
    for other in ys:
        pl.semaphore_signal(barrier, inc=1, device_id={"tp": other}, device_id_type=MESH)
    for dz in range(-NEAR, NEAR + 1):
        for q in range(NQ):
            if dz or q:
                pl.semaphore_signal(barrier, inc=1, device_id=at(dz, q), device_id_type=MESH)

    def hear(level):
        if level == 0:
            pl.semaphore_wait(barrier, (2 * NEAR + 1) * NQ - 1 + NY - 1)
        else:
            pl.semaphore_wait(wide_sem.at[level - 1], 2)
        reach = NEAR << level
        if reach < NZ // 2:
            for dz in (reach, -reach):
                pl.semaphore_signal(wide_sem.at[level], inc=1, device_id=at(dz, 0), device_id_type=MESH)

    loads = [
        pltpu.make_async_copy(ids_hbm, ids, load_sem.at[0]),
        pltpu.make_async_copy(tokens_hbm, tokens, load_sem.at[1]),
        pltpu.make_async_copy(pre_hbm, pre, load_sem.at[2]),
        pltpu.make_async_copy(weights_hbm, weights, load_sem.at[3]),
        pltpu.make_async_copy(gate_hbm.at[0], gate_up.at[:, pl.ds(0, LANES)], load_sem.at[4]),
        pltpu.make_async_copy(up_hbm.at[0], gate_up.at[:, pl.ds(LANES, LANES)], load_sem.at[5]),
        pltpu.make_async_copy(down_hbm.at[0], down, load_sem.at[6]),
    ]
    for load in loads:
        load.start()

    rows = tokens.shape[0]
    square_shape = (rows, rows)
    earlier_than = (iota(square_shape, 0) < iota(square_shape, 1)).astype(BF16)
    loads[0].wait()
    spots, before = [], None
    for k in range(2):
        e = ids[k : k + 1, :]
        dz = ((e >> 3) - z) & (NZ - 1)
        n = sum(jnp.where(dz == STEPS[i] % NZ, i, 0) for i in range(NZ))
        q = (((((e >> 1) & 3) - x) & 3) << 1) + (((e & 1) - c) & 1)
        p = n * NQ + q
        mark = (iota((PEERS, rows), 0) == p).astype(F32)
        earlier = dot(mark.astype(BF16), earlier_than)
        if before is not None:
            earlier = earlier + before
        before = jnp.sum(mark, axis=1, keepdims=True)
        slot = jnp.sum(earlier * mark, axis=0, keepdims=True)
        spots.append(p * BLOCK + slot.astype(I32))
    across = [jnp.concatenate([spot + CAP * part for part in range(PARTS)], axis=1) for spot in spots]

    loads[1].wait()
    loads[2].wait()
    values = tokens[...].astype(F32)
    scale = lax.rsqrt(jnp.mean(values * values, axis=1, keepdims=True) + epsilon)
    width = PARTS * LANES
    mine = pl.ds(pl.multiple_of(y * width, width), width)
    normed = (tokens[:, mine].astype(F32) * scale * pre[:, mine]).astype(BF16)
    stacked = jnp.concatenate([normed[:, part * LANES : (part + 1) * LANES] for part in range(PARTS)], axis=0)

    flat_sent = sent.reshape(PEERS * BLOCK, LANES)
    flat_arrived = arrived.reshape(PEERS * BLOCK, LANES)
    flat_results = results.reshape(PEERS * BLOCK, LANES)
    flat_returned = returned.reshape(PEERS * BLOCK, LANES)
    own_chunk, own = STEPS.index(0) // 2, STEPS.index(0) * NQ * CAP

    def send_blocks(source, target, sends, receives, j, place):
        for b in range(PER):
            n, q = divmod(j * PER + b, NQ)
            if not (STEPS[n] or q):
                continue
            rows_at = pl.ds((j * PER + b) * CAP, CAP)
            pltpu.make_async_remote_copy(
                source.at[rows_at], target.at[rows_at], sends.at[j], receives.at[j],
                device_id=place(n, q), device_id_type=MESH,
            ).start()
        if j == own_chunk:
            target[own : own + CAP] = source[own : own + CAP]

    def wait_blocks(buffer, sem, j):
        part = buffer.at[pl.ds(0, ROWS - CAP if j == own_chunk else ROWS)]
        pltpu.make_async_copy(part, part, sem.at[j]).wait()

    def send_tp(buffer, sends, receives, j):
        for other in ys:
            pltpu.make_async_remote_copy(
                buffer.at[j, y], buffer.at[j, y], sends.at[j], receives.at[j],
                device_id={"tp": other}, device_id_type=MESH,
            ).start()

    def wait_tp(buffer, sem, j):
        part = buffer.at[j, pl.ds(0, NY - 1)]
        pltpu.make_async_copy(part, part, sem.at[j]).wait()

    def assemble(j):
        r = iota((TALL, rows * PARTS), 0) + j * TALL
        take = jnp.where((r == across[0]) | (r == across[1]), 1.0, 0.0).astype(BF16)
        flat_sent[j * TALL : (j + 1) * TALL, :] = dot(take, stacked).astype(BF16)

    def send(j):
        if j + 1 < CHUNKS:
            assemble(j + 1)
        send_blocks(sent, arrived, out_sem, in_sem, j, ahead)

    to_wide = (iota((TALL, TALL), 1) == tall_row(iota((TALL, TALL), 0))).astype(BF16)
    to_tall = (iota((TALL, TALL), 0) == tall_row(iota((TALL, TALL), 1))).astype(BF16)

    def collect(j):
        wait_blocks(arrived, in_sem, j)
        wide = dot(to_wide, flat_arrived[j * TALL : (j + 1) * TALL, :]).astype(BF16)
        wide = jnp.concatenate([wide[part * ROWS : (part + 1) * ROWS] for part in range(PARTS)], axis=1)
        gathered[j, y] = wide
        send_tp(gathered, feat_out, feat_in, j)

    def gated(j):
        if j == 0:
            for load in loads[3:]:
                load.wait()
        wait_tp(gathered, feat_in, j)
        total = sum(dot(gathered[j, other], gate_up[other * width : (other + 1) * width, :]) for other in range(NY))
        gate, up = total[:, :LANES], total[:, LANES:]
        hidden[j, y] = (gate / (1.0 + jnp.exp(-gate)) * up).astype(BF16)
        send_tp(hidden, hid_out, hid_in, j)

    def project(j):
        wait_tp(hidden, hid_in, j)
        units = jnp.concatenate([hidden[j, other] for other in range(NY)], axis=1)
        made = dot(units, down[...]).astype(BF16)
        made = jnp.concatenate([made[:, part * LANES : (part + 1) * LANES] for part in range(PARTS)], axis=0)
        flat_results[j * TALL : (j + 1) * TALL, :] = dot(to_tall, made).astype(BF16)
        send_blocks(results, returned, ret_out, ret_in, j, behind)

    def column(row):
        return jnp.transpose(jnp.broadcast_to(row, square_shape))[:, 0:1]

    columns = []

    def merge(j):
        if not columns:
            columns.extend((column(spots[k].astype(F32)).astype(I32), column(weights[k : k + 1, :])) for k in range(2))
        r = iota((rows, TALL), 1) + j * TALL
        share = jnp.concatenate(
            [sum(jnp.where(r == s + CAP * part, w, 0.0) for s, w in columns) for part in range(PARTS)], axis=0
        )
        coarse = share.astype(BF16)
        fine = (share - coarse.astype(F32)).astype(BF16)
        wait_blocks(returned, ret_in, j)
        back = flat_returned[j * TALL : (j + 1) * TALL, :]
        added = dot(coarse, back) + dot(fine, back)
        mixed[...] = added if j == 0 else mixed[...] + added

    assemble(0)
    steps = dict(K=hear, S=send, C=collect, G=gated, P=project, M=merge)
    for step in PLAN:
        steps[step[0]](int(step[1:]))

    pieces = [mixed[part * rows : (part + 1) * rows, :] for part in range(PARTS)]
    square = jnp.sum(sum(piece * piece for piece in pieces), axis=1, keepdims=True)
    squares[y] = jnp.transpose(jnp.broadcast_to(square, square_shape))[0:1, :]
    for other in ys:
        pltpu.make_async_remote_copy(
            squares.at[y], squares.at[y], sq_sem.at[0], sq_sem.at[1], device_id={"tp": other}, device_id_type=MESH
        ).start()
    for j in range(CHUNKS):
        wait_blocks(sent, out_sem, j)
        wait_blocks(results, ret_out, j)
        wait_tp(gathered, feat_out, j)
        wait_tp(hidden, hid_out, j)
    three = squares.at[pl.ds(0, NY - 1)]
    pltpu.make_async_copy(three, three, sq_sem.at[1]).wait()
    total = squares[0] + squares[1] + squares[2] + squares[3]
    out_scale = lax.rsqrt(total / (width * NY) + epsilon)
    out_scale = jnp.transpose(jnp.broadcast_to(out_scale, square_shape))
    for part in range(PARTS):
        o_ref[:, part * LANES : (part + 1) * LANES] = pieces[part] * out_scale
    pltpu.make_async_copy(three, three, sq_sem.at[0]).wait()


def per_device(tokens, pre_gain, post_gain, expert_ids, route_weights, w_gate, w_up, w_down):
    rows, row_width = tokens.shape
    width = PARTS * LANES
    blocks = pltpu.VMEM((PEERS * CAP, PARTS, LANES), BF16)
    sems = pltpu.SemaphoreType.DMA((CHUNKS,))
    scaled = pl.pallas_call(
        kernel,
        out_shape=pltpu.VMEM((rows, width), F32),
        in_specs=[pl.BlockSpec(memory_space=pltpu.HBM)] * 7,
        out_specs=pl.BlockSpec(memory_space=pltpu.VMEM),
        scratch_shapes=[
            pltpu.VMEM((rows, row_width), BF16),
            pltpu.VMEM((1, row_width), F32),
            pltpu.VMEM((2, rows), I32),
            pltpu.VMEM((2, rows), F32),
            pltpu.VMEM((row_width, 2 * LANES), BF16),
            pltpu.VMEM((w_down.shape[1], width), BF16),
            blocks,
            blocks,
            pltpu.VMEM((CHUNKS, NY, ROWS, width), BF16),
            pltpu.VMEM((CHUNKS, NY, ROWS, LANES), BF16),
            blocks,
            blocks,
            pltpu.VMEM((NY, 1, rows), F32),
            pltpu.VMEM((rows * PARTS, LANES), F32),
            pltpu.SemaphoreType.DMA((7,)),
            pltpu.SemaphoreType.REGULAR((3,)),
            *[sems] * 8,
            pltpu.SemaphoreType.DMA((2,)),
        ],
        compiler_params=pltpu.CompilerParams(
            collective_id=0, has_side_effects=True
        ),
    )(tokens, pre_gain[None, :], expert_ids.T, route_weights.T, w_gate, w_up, w_down)
    return (scaled * post_gain[None, :]).astype(BF16)


def solution(mesh):
    in_specs = (
        P("ep", None),
        P(),
        P("tp"),
        P("ep", None),
        P("ep", None),
        P("ep", None, "tp"),
        P("ep", None, "tp"),
        P("ep", None, "tp"),
    )
    return jax.shard_map(per_device, mesh=mesh, in_specs=in_specs, out_specs=P("ep", "tp"), check_vma=False)
```

time: 76.3 us -> 68 us (0.89)
  Pallas kernels: 72.3 us -> 67.2 us
  local copies, waits for them, and re-layouts: 3.72 us -> 0.01 us
    pallas_call x1, Pallas kernels: 72.3 us -> 67.2 us  [per_device(): pl.pallas_call(kernel, out_shape=pltpu.VMEM((rows, width), F32), in_specs...]
    unnamed x7 -> x2, local copies, waits for them, and re-layouts: 3.72 us -> 0.01 us
where the time goes in v3:
time: 68 us; the launch traced here: 67.9 us
  Pallas kernels  67.2 us (99%)
  other arithmetic  0.68 us (1%)
    pallas_call x1, Pallas kernels, per_device(): pl.pallas_call(kernel, out_shape=pltpu.VMEM((rows, width), F32), in_specs...  67.2 us

profile of v3, /device:TPU:1, one launch (start us, length us, event | category | flops | bytes accessed | tf_op | source)
XLA Modules:
  0.0 67.9 jit_solution(2641462328819047380)
XLA Ops:
  0.0 0.0 copy-start
  0.0 67.2 %shard_map.82 = f32[128,512]{1,0:T(8,128)S(1)} custom-call(bf16[128,2048]{1,0:T(8,128)(2,1)} %tokens_hbm.1, f32[1,2048]{1,0:T(1,128)} %bitcast.3, s32[2,128]{1,0:T(2,128)} %bitcast.4, f32[2,128]{1,0:T(2,128)} %bitcast.5, bf16[1,2048,128]{2,1,0:T(8,128)(2,1)} %gate_hbm.1, bf16[1,2048,128]{2,1,0:T(8,128)(2,1)} %up_hbm.1, bf16[1,512,512]{2,1,0:T(8,128)(2,1)} %down_hbm.1), custom_call_target="tpu_custom_call" | custom-call | tf_op jit(solution)/shard_map/pallas_call | solution.py:250
  67.2 0.0 copy-done
  67.2 0.7 multiply_convert_fusion
Async XLA Ops:
  0.0 67.2 %copy-start = (f32[512]{0:T(512)S(1)}, f32[512]{0:T(512)}, u32[]{:S(2)}) copy-start(f32[512]{0:T(512)} %param.10) | copy-start | bytes 6148

commit v4 on v3

--- a/solution.py
+++ b/solution.py
@@ -10,21 +10,24 @@
 NZ, NX, NC, NY = 16, 4, 2, 4
 NQ = NX * NC
 PEERS = NZ * NQ
+FARTHEST = (5, 4, 3, 7, 2, 6, 1, 0)
 CAP = 3
-STEPS = (0, 1, -1, 2, -2, 3, -3, 4, 8, -7, 7, -6, 6, -5, 5, -4)
+STEPS = (0, 1, -1, 2, -2, 3, 4, -4, -3, 8, -7, 7, -6, 6, -5, 5)
 PLAN = (
-    "K0", "S0", "S1", "K1", "S2", "S3", "K2", "S4", "S5", "S6", "S7", "C0", "C1", "C2", "C3", "G0", "G1", "G2",
-    "G3", "P0", "C4", "P1", "P2", "P3", "C5", "G4", "C6", "G5", "P4", "C7", "G6", "P5", "G7", "P6", "P7", "M0",
-    "M1", "M2", "M3", "M4", "M5", "M6", "M7",
+    "A0", "A1", "A2", "A3", "K0", "S0", "S1", "A4", "A5", "K1", "S2", "S3", "A6", "A7", "K2", "S4", "S5", "S6",
+    "S7", "C0", "C1", "C2", "C3", "G0", "G1", "G2", "G3", "P0", "C4", "P1", "P2", "C5", "P3", "G4", "C6", "G5",
+    "P4", "C7", "G6", "P5", "G7", "P6", "P7", "M0", "M1", "M2", "M3", "M4", "M5", "M6", "M7",
 )
 NEAR = 2
-CHUNKS = 8
-PER = PEERS // CHUNKS
-ROWS = PER * CAP
+EDGES = (0, 2, 4, 6, 8, 10, 12, 14, 16)
+CHUNKS = len(EDGES) - 1
+SPAN = [EDGES[j + 1] - EDGES[j] for j in range(CHUNKS)]
+ROWS = [NQ * CAP * span for span in SPAN]
 LANES = 128
 PARTS = 4
 BLOCK = PARTS * CAP
-TALL = PER * BLOCK
+TALL = [NQ * BLOCK * span for span in SPAN]
+BASE = [NQ * BLOCK * edge for edge in EDGES]
 BF16, F32, I32 = jnp.bfloat16, jnp.float32, jnp.int32
 
 
@@ -36,9 +39,9 @@
     return lax.broadcasted_iota(I32, shape, dim)
 
 
-def tall_row(wide):
-    part = sum((wide >= ROWS * k).astype(I32) for k in range(1, PARTS))
-    rest = wide - part * ROWS
+def tall_row(wide, rows):
+    part = sum((wide >= rows * k).astype(I32) for k in range(1, PARTS))
+    rest = wide - part * rows
     block = (rest * 171) >> 9
     return block * BLOCK + part * CAP + (rest - block * CAP)
 
@@ -46,15 +49,16 @@
 def kernel(
     tokens_hbm, pre_hbm, ids_hbm, weights_hbm, gate_hbm, up_hbm, down_hbm,
     o_ref,
-    tokens, pre, ids, weights, gate_up, down, sent, arrived, gathered, hidden, results, returned, squares, mixed,
-    load_sem, wide_sem, out_sem, in_sem, feat_out, feat_in, hid_out, hid_in, ret_out, ret_in, sq_sem,
+    tokens, pre, ids, weights, gate_up, down, sent, arrived, results, returned, squares, mixed,
+    load_sem, wide_sem, out_sem, in_sem, feat_out, feat_in, hid_out, hid_in, ret_out, ret_in, sq_sem, *buffers,
 ):
+    gathered, hidden = buffers[:CHUNKS], buffers[CHUNKS:]
     me, y = lax.axis_index("ep"), lax.axis_index("tp")
     z, x, c = lax.div(me, NQ), lax.rem(lax.div(me, NC), NX), lax.rem(me, NC)
     zs = [lax.rem(z + d, NZ) * NQ for d in range(NZ)]
     xs = [lax.rem(x + d, NX) * NC for d in range(NX)]
     cs = [c, 1 - c]
-    ys = [lax.rem(y + d, NY) for d in (1, 3, 2)]
+    ys = [lax.rem(y + d, NY) for d in (2, 1, 3)]
 
     def at(dz, q):
         return {"ep": zs[dz % NZ] + xs[q // NC] + cs[q % NC]}
@@ -68,14 +72,15 @@
     barrier = pltpu.get_barrier_semaphore()
     for other in ys:
         pl.semaphore_signal(barrier, inc=1, device_id={"tp": other}, device_id_type=MESH)
-    for dz in range(-NEAR, NEAR + 1):
-        for q in range(NQ):
+    near = range(max(-NEAR, 1 - NZ // 2), NEAR + 1)
+    for dz in sorted(near, key=abs, reverse=True):
+        for q in FARTHEST:
             if dz or q:
                 pl.semaphore_signal(barrier, inc=1, device_id=at(dz, q), device_id_type=MESH)
 
     def hear(level):
         if level == 0:
-            pl.semaphore_wait(barrier, (2 * NEAR + 1) * NQ - 1 + NY - 1)
+            pl.semaphore_wait(barrier, len(near) * NQ - 1 + NY - 1)
         else:
             pl.semaphore_wait(wide_sem.at[level - 1], 2)
         reach = NEAR << level
@@ -128,14 +133,14 @@
     flat_arrived = arrived.reshape(PEERS * BLOCK, LANES)
     flat_results = results.reshape(PEERS * BLOCK, LANES)
     flat_returned = returned.reshape(PEERS * BLOCK, LANES)
-    own_chunk, own = STEPS.index(0) // 2, STEPS.index(0) * NQ * CAP
+    own = STEPS.index(0) * NQ * CAP
+    own_chunk = max(j for j in range(CHUNKS) if EDGES[j] <= STEPS.index(0))
 
     def send_blocks(source, target, sends, receives, j, place):
-        for b in range(PER):
-            n, q = divmod(j * PER + b, NQ)
+        for q, n in ((q, n) for q in FARTHEST for n in range(EDGES[j], EDGES[j + 1])):
             if not (STEPS[n] or q):
                 continue
-            rows_at = pl.ds((j * PER + b) * CAP, CAP)
+            rows_at = pl.ds((n * NQ + q) * CAP, CAP)
             pltpu.make_async_remote_copy(
                 source.at[rows_at], target.at[rows_at], sends.at[j], receives.at[j],
                 device_id=place(n, q), device_id_type=MESH,
@@ -144,38 +149,42 @@
             target[own : own + CAP] = source[own : own + CAP]
 
     def wait_blocks(buffer, sem, j):
-        part = buffer.at[pl.ds(0, ROWS - CAP if j == own_chunk else ROWS)]
+        part = buffer.at[pl.ds(0, ROWS[j] - CAP if j == own_chunk else ROWS[j])]
         pltpu.make_async_copy(part, part, sem.at[j]).wait()
 
     def send_tp(buffer, sends, receives, j):
         for other in ys:
             pltpu.make_async_remote_copy(
-                buffer.at[j, y], buffer.at[j, y], sends.at[j], receives.at[j],
+                buffer[j].at[y], buffer[j].at[y], sends.at[j], receives.at[j],
                 device_id={"tp": other}, device_id_type=MESH,
             ).start()
 
     def wait_tp(buffer, sem, j):
-        part = buffer.at[j, pl.ds(0, NY - 1)]
+        part = buffer[j].at[pl.ds(0, NY - 1)]
         pltpu.make_async_copy(part, part, sem.at[j]).wait()
 
     def assemble(j):
-        r = iota((TALL, rows * PARTS), 0) + j * TALL
+        r = iota((TALL[j], rows * PARTS), 0) + BASE[j]
         take = jnp.where((r == across[0]) | (r == across[1]), 1.0, 0.0).astype(BF16)
-        flat_sent[j * TALL : (j + 1) * TALL, :] = dot(take, stacked).astype(BF16)
+        flat_sent[BASE[j] : BASE[j + 1], :] = dot(take, stacked).astype(BF16)
 
     def send(j):
-        if j + 1 < CHUNKS:
-            assemble(j + 1)
         send_blocks(sent, arrived, out_sem, in_sem, j, ahead)
 
-    to_wide = (iota((TALL, TALL), 1) == tall_row(iota((TALL, TALL), 0))).astype(BF16)
-    to_tall = (iota((TALL, TALL), 0) == tall_row(iota((TALL, TALL), 1))).astype(BF16)
+    order = {}
+    for tall, count in dict(zip(TALL, ROWS)).items():
+        shape = (tall, tall)
+        order[tall] = (
+            (iota(shape, 1) == tall_row(iota(shape, 0), count)).astype(BF16),
+            (iota(shape, 0) == tall_row(iota(shape, 1), count)).astype(BF16),
+        )
 
     def collect(j):
         wait_blocks(arrived, in_sem, j)
-        wide = dot(to_wide, flat_arrived[j * TALL : (j + 1) * TALL, :]).astype(BF16)
-        wide = jnp.concatenate([wide[part * ROWS : (part + 1) * ROWS] for part in range(PARTS)], axis=1)
-        gathered[j, y] = wide
+        wide = dot(order[TALL[j]][0], flat_arrived[BASE[j] : BASE[j + 1], :])
+        n = ROWS[j]
+        wide = jnp.concatenate([wide[part * n : (part + 1) * n] for part in range(PARTS)], axis=1)
+        gathered[j][y] = wide.astype(BF16)
         send_tp(gathered, feat_out, feat_in, j)
 
     def gated(j):
@@ -183,17 +192,17 @@
             for load in loads[3:]:
                 load.wait()
         wait_tp(gathered, feat_in, j)
-        total = sum(dot(gathered[j, other], gate_up[other * width : (other + 1) * width, :]) for other in range(NY))
+        total = sum(dot(gathered[j][other], gate_up[other * width : (other + 1) * width, :]) for other in range(NY))
         gate, up = total[:, :LANES], total[:, LANES:]
-        hidden[j, y] = (gate / (1.0 + jnp.exp(-gate)) * up).astype(BF16)
+        hidden[j][y] = (gate / (1.0 + jnp.exp(-gate)) * up).astype(BF16)
         send_tp(hidden, hid_out, hid_in, j)
 
     def project(j):
         wait_tp(hidden, hid_in, j)
-        units = jnp.concatenate([hidden[j, other] for other in range(NY)], axis=1)
-        made = dot(units, down[...]).astype(BF16)
+        units = jnp.concatenate([hidden[j][other] for other in range(NY)], axis=1)
+        made = dot(units, down[...])
         made = jnp.concatenate([made[:, part * LANES : (part + 1) * LANES] for part in range(PARTS)], axis=0)
-        flat_results[j * TALL : (j + 1) * TALL, :] = dot(to_tall, made).astype(BF16)
+        flat_results[BASE[j] : BASE[j + 1], :] = dot(order[TALL[j]][1], made.astype(BF16)).astype(BF16)
         send_blocks(results, returned, ret_out, ret_in, j, behind)
 
     def column(row):
@@ -202,21 +211,21 @@
     columns = []
 
     def merge(j):
-        if not columns:
+        first = not columns
+        if first:
             columns.extend((column(spots[k].astype(F32)).astype(I32), column(weights[k : k + 1, :])) for k in range(2))
-        r = iota((rows, TALL), 1) + j * TALL
+        r = iota((rows, TALL[j]), 1) + BASE[j]
         share = jnp.concatenate(
             [sum(jnp.where(r == s + CAP * part, w, 0.0) for s, w in columns) for part in range(PARTS)], axis=0
         )
         coarse = share.astype(BF16)
         fine = (share - coarse.astype(F32)).astype(BF16)
         wait_blocks(returned, ret_in, j)
-        back = flat_returned[j * TALL : (j + 1) * TALL, :]
+        back = flat_returned[BASE[j] : BASE[j + 1], :]
         added = dot(coarse, back) + dot(fine, back)
-        mixed[...] = added if j == 0 else mixed[...] + added
-
-    assemble(0)
-    steps = dict(K=hear, S=send, C=collect, G=gated, P=project, M=merge)
+        mixed[...] = added if first else mixed[...] + added
+
+    steps = dict(A=assemble, K=hear, S=send, C=collect, G=gated, P=project, M=merge)
     for step in PLAN:
         steps[step[0]](int(step[1:]))
 
@@ -261,8 +270,6 @@
             pltpu.VMEM((w_down.shape[1], width), BF16),
             blocks,
             blocks,
-            pltpu.VMEM((CHUNKS, NY, ROWS, width), BF16),
-            pltpu.VMEM((CHUNKS, NY, ROWS, LANES), BF16),
             blocks,
             blocks,
             pltpu.VMEM((NY, 1, rows), F32),
@@ -271,6 +278,8 @@
             pltpu.SemaphoreType.REGULAR((3,)),
             *[sems] * 8,
             pltpu.SemaphoreType.DMA((2,)),
+            *[pltpu.VMEM((NY, count, width), BF16) for count in ROWS],
+            *[pltpu.VMEM((NY, count, LANES), BF16) for count in ROWS],
         ],
         compiler_params=pltpu.CompilerParams(
             collective_id=0, has_side_effects=True

time: 68 us -> 63.3 us (0.931)
  Pallas kernels: 67.2 us -> 62.4 us
    pallas_call x1, Pallas kernels: 67.2 us -> 62.4 us  [per_device(): pl.pallas_call(kernel, out_shape=pltpu.VMEM((rows, width), F32), in_specs...]
where the time goes in v4:
time: 63.3 us; the launch traced here: 63.1 us
  Pallas kernels  62.4 us (99%)
  other arithmetic  0.68 us (1%)
    pallas_call x1, Pallas kernels, per_device(): pl.pallas_call(kernel, out_shape=pltpu.VMEM((rows, width), F32), in_specs...  62.4 us

profile of v4, /device:TPU:1, one launch (start us, length us, event | category | flops | bytes accessed | tf_op | source)
XLA Modules:
  0.0 63.1 jit_solution(12016695539610903150)
XLA Ops:
  0.0 0.0 copy-start
  0.0 62.4 %shard_map.82 = f32[128,512]{1,0:T(8,128)S(1)} custom-call(bf16[128,2048]{1,0:T(8,128)(2,1)} %tokens_hbm.1, f32[1,2048]{1,0:T(1,128)} %bitcast.3, s32[2,128]{1,0:T(2,128)} %bitcast.4, f32[2,128]{1,0:T(2,128)} %bitcast.5, bf16[1,2048,128]{2,1,0:T(8,128)(2,1)} %gate_hbm.1, bf16[1,2048,128]{2,1,0:T(8,128)(2,1)} %up_hbm.1, bf16[1,512,512]{2,1,0:T(8,128)(2,1)} %down_hbm.1), custom_call_target="tpu_custom_call" | custom-call | tf_op jit(solution)/shard_map/pallas_call | solution.py:259
  62.4 0.0 copy-done
  62.5 0.7 %multiply_convert_fusion = bf16[128,512]{1,0:T(8,128)(2,1)} fusion(f32[128,512]{1,0:T(8,128)S(1)} %shard_map.82, f32[512]{0:T(512)S(1)} %copy-done), kind=kLoop, calls=%fused_computation | loop fusion | flops 131072 | bytes 395264 | tf_op jit(solution)/shard_map/convert_element_type | solution.py:288
Async XLA Ops:
  0.0 62.4 %copy-start = (f32[512]{0:T(512)S(1)}, f32[512]{0:T(512)}, u32[]{:S(2)}) copy-start(f32[512]{0:T(512)} %param.10) | copy-start | bytes 6148

commit v5 on v4

--- a/solution.py
+++ b/solution.py
@@ -14,8 +14,8 @@
 CAP = 3
 STEPS = (0, 1, -1, 2, -2, 3, 4, -4, -3, 8, -7, 7, -6, 6, -5, 5)
 PLAN = (
-    "A0", "A1", "A2", "A3", "K0", "S0", "S1", "A4", "A5", "K1", "S2", "S3", "A6", "A7", "K2", "S4", "S5", "S6",
-    "S7", "C0", "C1", "C2", "C3", "G0", "G1", "G2", "G3", "P0", "C4", "P1", "P2", "C5", "P3", "G4", "C6", "G5",
+    "A0", "A1", "A2", "A3", "K0", "S0", "S1", "A4", "A5", "K1", "S2", "S3", "A6", "A7", "C0", "K2", "S4", "S5",
+    "S6", "S7", "C1", "C2", "C3", "G0", "G1", "G2", "G3", "P0", "P1", "C4", "P2", "C5", "P3", "G4", "C6", "G5",
     "P4", "C7", "G6", "P5", "G7", "P6", "P7", "M0", "M1", "M2", "M3", "M4", "M5", "M6", "M7",
 )
 NEAR = 2

time: 63.3 us -> 62.9 us (level)
  no operation moved by 1% of the time
where the time goes in v5:
time: 62.9 us; the launch traced here: 62.7 us
  Pallas kernels  62 us (99%)
  other arithmetic  0.68 us (1%)
    pallas_call x1, Pallas kernels, per_device(): pl.pallas_call(kernel, out_shape=pltpu.VMEM((rows, width), F32), in_specs...  62 us

profile of v5, /device:TPU:1, one launch (start us, length us, event | category | flops | bytes accessed | tf_op | source)
XLA Modules:
  0.0 62.7 jit_solution(9943077853033491430)
XLA Ops:
  0.0 0.0 copy-start
  0.0 62.0 %shard_map.82 = f32[128,512]{1,0:T(8,128)S(1)} custom-call(bf16[128,2048]{1,0:T(8,128)(2,1)} %tokens_hbm.1, f32[1,2048]{1,0:T(1,128)} %bitcast.3, s32[2,128]{1,0:T(2,128)} %bitcast.4, f32[2,128]{1,0:T(2,128)} %bitcast.5, bf16[1,2048,128]{2,1,0:T(8,128)(2,1)} %gate_hbm.1, bf16[1,2048,128]{2,1,0:T(8,128)(2,1)} %up_hbm.1, bf16[1,512,512]{2,1,0:T(8,128)(2,1)} %down_hbm.1), custom_call_target="tpu_custom_call" | custom-call | tf_op jit(solution)/shard_map/pallas_call | solution.py:259
  62.0 0.0 copy-done
  62.0 0.7 %multiply_convert_fusion = bf16[128,512]{1,0:T(8,128)(2,1)} fusion(f32[128,512]{1,0:T(8,128)S(1)} %shard_map.82, f32[512]{0:T(512)S(1)} %copy-done), kind=kLoop, calls=%fused_computation | loop fusion | flops 131072 | bytes 395264 | tf_op jit(solution)/shard_map/convert_element_type | solution.py:288
Async XLA Ops:
  0.0 62.0 %copy-start = (f32[512]{0:T(512)S(1)}, f32[512]{0:T(512)}, u32[]{:S(2)}) copy-start(f32[512]{0:T(512)} %param.10) | copy-start | bytes 6148

commit v6 on v5

--- a/solution.py
+++ b/solution.py
@@ -58,7 +58,7 @@
     zs = [lax.rem(z + d, NZ) * NQ for d in range(NZ)]
     xs = [lax.rem(x + d, NX) * NC for d in range(NX)]
     cs = [c, 1 - c]
-    ys = [lax.rem(y + d, NY) for d in (2, 1, 3)]
+    ys = [lax.rem(y + d, NY) for d in (2, 3, 1)]
 
     def at(dz, q):
         return {"ep": zs[dz % NZ] + xs[q // NC] + cs[q % NC]}

time: 62.9 us -> 62.9 us (level)
  no operation moved by 1% of the time
where the time goes in v6:
time: 62.9 us; the launch traced here: 62.7 us
  Pallas kernels  62 us (99%)
  other arithmetic  0.68 us (1%)
    pallas_call x1, Pallas kernels, per_device(): pl.pallas_call(kernel, out_shape=pltpu.VMEM((rows, width), F32), in_specs...  62 us

profile of v6, /device:TPU:1, one launch (start us, length us, event | category | flops | bytes accessed | tf_op | source)
XLA Modules:
  0.0 62.7 jit_solution(13033896288581772941)
XLA Ops:
  0.0 0.0 copy-start
  0.0 62.0 %shard_map.82 = f32[128,512]{1,0:T(8,128)S(1)} custom-call(bf16[128,2048]{1,0:T(8,128)(2,1)} %tokens_hbm.1, f32[1,2048]{1,0:T(1,128)} %bitcast.3, s32[2,128]{1,0:T(2,128)} %bitcast.4, f32[2,128]{1,0:T(2,128)} %bitcast.5, bf16[1,2048,128]{2,1,0:T(8,128)(2,1)} %gate_hbm.1, bf16[1,2048,128]{2,1,0:T(8,128)(2,1)} %up_hbm.1, bf16[1,512,512]{2,1,0:T(8,128)(2,1)} %down_hbm.1), custom_call_target="tpu_custom_call" | custom-call | tf_op jit(solution)/shard_map/pallas_call | solution.py:259
  62.0 0.0 copy-done
  62.0 0.7 %multiply_convert_fusion = bf16[128,512]{1,0:T(8,128)(2,1)} fusion(f32[128,512]{1,0:T(8,128)S(1)} %shard_map.82, f32[512]{0:T(512)S(1)} %copy-done), kind=kLoop, calls=%fused_computation | loop fusion | flops 131072 | bytes 395264 | tf_op jit(solution)/shard_map/convert_element_type | solution.py:288
Async XLA Ops:
  0.0 62.0 %copy-start = (f32[512]{0:T(512)S(1)}, f32[512]{0:T(512)}, u32[]{:S(2)}) copy-start(f32[512]{0:T(512)} %param.10) | copy-start | bytes 6148
